TPU v7x, 32 devices: a whole 2x2x4 slice. The times are simulated.
32 devices in a mesh: fs: 8 (over z, y), tp: 4 (over x, core).
Axes of the slice: x: 2, y: 2, z: 4, core: 2. Of those that a mesh axis runs over, the one named last changes fastest.
Arguments:
- x_next: bfloat16 [1536, 2048], P(('fs', 'tp')), may hold values from -6 to 6
- x_prev: bfloat16 [1536, 2048], P(('fs', 'tp')), may hold values from -6 to 6
- grad_out: bfloat16 [1536, 2048], P(('fs', 'tp')), may hold values from -6 to 6
- gate_w: bfloat16 [2048, 2816], P('fs', 'tp'), may hold values from -0.125 to 0.125
- up_w: bfloat16 [2048, 2816], P('fs', 'tp'), may hold values from -0.125 to 0.125
- down_w: bfloat16 [2816, 2048], P('tp', 'fs'), may hold values from -0.109375 to 0.109375
- acc_gate: float32 [2048, 2816], P('fs', 'tp'), may hold values from -2.5 to 2.5
- acc_up: float32 [2048, 2816], P('fs', 'tp'), may hold values from -2.5 to 2.5
- acc_down: float32 [2816, 2048], P('tp', 'fs'), may hold values from -2.5 to 2.5
Outputs:
- out_next: bfloat16 [1536, 2048], P(('fs', 'tp'))
- saved_hidden: bfloat16 [1536, 2816], P('fs', 'tp')
- grad_input: bfloat16 [1536, 2048], P(('fs', 'tp'))
- new_gate: float32 [2048, 2816], P('fs', 'tp')
- new_up: float32 [2048, 2816], P('fs', 'tp')
- new_down: float32 [2816, 2048], P('tp', 'fs')
All inputs are finite; a program needn't handle non-finite values.
Results may differ from a plain program's by a relative error of at most 0.014.
Values may be sent and summed in bfloat16 or wider, within the bound.
A program may use at most 64 MiB of HBM per device.

v0:
```python
import math

import jax
import jax.numpy as jnp
from jax import lax
from jax.sharding import PartitionSpec as P


def contract_rows(left, right):
    return lax.dot_general(
        left, right, (((0,), (0,)), ((), ())), preferred_element_type=jnp.float32
    )


def contract_cols(left, right):
    return lax.dot_general(
        left, right, (((1,), (1,)), ((), ())), preferred_element_type=jnp.float32
    )


def local(x_next, x_prev, grad_out, gate_w, up_w, down_w, acc_gate, acc_up, acc_down):
    local_rows = x_prev.shape[0]
    total_rows = local_rows * lax.axis_size("tp") * lax.axis_size("fs")
    factor = 1.0 / math.sqrt(total_rows)
    kept = (
        lax.all_gather(gate_w, "fs", axis=0, tiled=True),
        lax.all_gather(up_w, "fs", axis=0, tiled=True),
        lax.all_gather(down_w, "fs", axis=1, tiled=True),
    )
    gate_full, up_full, down_full = kept
    piece = lax.all_gather(x_next, "tp", axis=0, tiled=True)
    gate = jnp.dot(piece, gate_full, preferred_element_type=jnp.float32)
    upper = jnp.dot(piece, up_full, preferred_element_type=jnp.float32)
    hidden = (jax.nn.silu(gate) * upper).astype(jnp.bfloat16)
    summed = lax.psum_scatter(
        jnp.dot(hidden, down_full, preferred_element_type=jnp.float32).astype(jnp.bfloat16),
        "tp",
        scatter_dimension=0,
        tiled=True,
    )
    backward_gate_full, backward_up_full, backward_down_full = kept
    rows_prev = lax.all_gather(x_prev, "tp", axis=0, tiled=True)
    cotangent = lax.all_gather(grad_out, "tp", axis=0, tiled=True)
    gate_prev = jnp.dot(rows_prev, backward_gate_full, preferred_element_type=jnp.float32)
    up_prev = jnp.dot(rows_prev, backward_up_full, preferred_element_type=jnp.float32)
    grad_hidden = contract_cols(cotangent, backward_down_full)
    sigmoid_gate = jax.nn.sigmoid(gate_prev)
    silu_gate = gate_prev * sigmoid_gate
    grad_gate = (
        grad_hidden * up_prev * sigmoid_gate * (1.0 + gate_prev * (1.0 - sigmoid_gate))
    ).astype(jnp.bfloat16)
    grad_up = (grad_hidden * silu_gate).astype(jnp.bfloat16)
    hidden_prev = (silu_gate * up_prev).astype(jnp.bfloat16)
    columns = cotangent
    down_shard = lax.psum_scatter(
        contract_rows(columns, hidden_prev), "fs", scatter_dimension=0, tiled=True
    )
    new_down = acc_down + factor * down_shard.T
    stacked = jnp.concatenate((grad_gate, grad_up), axis=1)
    columns = rows_prev
    both_shard = lax.psum_scatter(
        contract_rows(columns, stacked), "fs", scatter_dimension=0, tiled=True
    )
    width = grad_gate.shape[1]
    new_gate = acc_gate + factor * both_shard[:, :width]
    new_up = acc_up + factor * both_shard[:, width:]
    first = contract_cols(grad_gate, backward_gate_full)
    second = contract_cols(grad_up, backward_up_full)
    grad_input = lax.psum_scatter(
        (first + second).astype(jnp.bfloat16), "tp", scatter_dimension=0, tiled=True
    )
    grad_input, new_gate, new_up, new_down = (grad_input, new_gate, new_up, new_down)
    return (summed, hidden, grad_input, new_gate, new_up, new_down)


def solution(mesh):
    in_specs = (
        P(("fs", "tp"), None),
        P(("fs", "tp"), None),
        P(("fs", "tp"), None),
        P("fs", "tp"),
        P("fs", "tp"),
        P("tp", "fs"),
        P("fs", "tp"),
        P("fs", "tp"),
        P("tp", "fs"),
    )
    out_specs = (
        P(("fs", "tp"), None),
        P("fs", "tp"),
        P(("fs", "tp"), None),
        P("fs", "tp"),
        P("fs", "tp"),
        P("tp", "fs"),
    )
    return jax.shard_map(local, mesh=mesh, in_specs=in_specs, out_specs=out_specs, check_vma=False)
```

profile of v0, /device:TPU:0, one launch (start us, length us, event | category | flops | bytes accessed | tf_op | source)
XLA Modules:
  0.0 559.3 jit_solution(16797564470461759762)
XLA Ops:
  7.2 0.7 all-gather.4.cloned.1.call-update
  7.9 0.7 all-gather.6.cloned.1.call-update
  8.7 0.7 all-gather.8.cloned.1.call-update
  9.4 0.0 reduce-scatter.11.cloned.1.call-start
  9.4 10.3 %all_gather.23 = bf16[192,2048]{1,0:T(8,128)(2,1)S(1)} all-gather(bf16[48,2048]{1,0:T(8,128)(2,1)} %param.10), channel_id=1, replica_groups=mesh['fs'=8,'tp'=4] {'tp'}, dimensions={0}, use_global_device_ids=true | all-gather | bytes 983040 | tf_op jit(solution)/shard_map/all_gather | solution.py:42
  19.7 8.9 %all_gather.22 = bf16[192,2048]{1,0:T(8,128)(2,1)S(1)} all-gather(bf16[48,2048]{1,0:T(8,128)(2,1)} %param.11), channel_id=1, replica_groups=mesh['fs'=8,'tp'=4] {'tp'}, dimensions={0}, use_global_device_ids=true | all-gather | bytes 983040 | tf_op jit(solution)/shard_map/all_gather | solution.py:43
  28.6 43.7 %all-gather.4.cloned.1.call-done = bf16[2048,704]{0,1:T(8,128)(2,1)} async-done(((bf16[256,704]{0,1:T(8,128)(2,1)}), bf16[2048,704]{0,1:T(8,128)(2,1)}) %all-gather.4.cloned.1.call-update) | async-done | bytes 2883600 | tf_op jit(solution)/shard_map/all_gather | solution.py:26
  72.3 2.8 fusion.13
  75.2 57.0 %all-gather.6.cloned.1.call-done = bf16[2048,704]{0,1:T(8,128)(2,1)} async-done(((bf16[256,704]{0,1:T(8,128)(2,1)}), bf16[2048,704]{0,1:T(8,128)(2,1)}) %all-gather.6.cloned.1.call-update) | async-done | bytes 2883600 | tf_op jit(solution)/shard_map/all_gather | solution.py:27
  132.1 2.8 fusion.12
  135.0 3.4 convolution_bitcast_fusion.1
  138.4 0.0 reduce-scatter.9.cloned.1.call-start
  138.5 53.5 %all-gather.8.cloned.1.call-done = bf16[704,2048]{1,0:T(8,128)(2,1)} async-done(((bf16[704,256]{1,0:T(8,128)(2,1)}), bf16[704,2048]{1,0:T(8,128)(2,1)}) %all-gather.8.cloned.1.call-update) | async-done | bytes 2883600 | tf_op jit(solution)/shard_map/all_gather | solution.py:28
  192.0 2.9 multiply_convert_fusion.1
  194.9 6.1 %convolution_bitcast_fusion = f32[2048,1408]{0,1:T(8,128)} fusion(bf16[192,2048]{1,0:T(8,128)(2,1)S(1)} %all_gather.23, bf16[192,704]{1,0:T(8,128)(2,1)S(1)} %get-tuple-element.8, bf16[192,704]{1,0:T(8,128)(2,1)S(1)} %get-tuple-element.9), kind=kOutput, calls=%fused_computation | convolution fusion | flops 1108377600 | bytes 12861440 | tf_op jit(solution)/shard_map/dot_general | solution.py:10
  201.1 0.0 reduce-scatter.7.cloned.1.call-start
  201.1 1.8 copy-done
  202.9 0.8 fusion.14
  203.7 1.0 copy-done.1
  204.7 1.7 fusion
  206.5 0.0 reduce-scatter.5.cloned.1.call-start
  206.5 8.8 %all_gather.18 = bf16[192,2048]{1,0:T(8,128)(2,1)S(1)} all-gather(bf16[48,2048]{1,0:T(8,128)(2,1)S(1)} %copy-done.8), channel_id=1, replica_groups=mesh['fs'=8,'tp'=4] {'tp'}, dimensions={0}, use_global_device_ids=true | all-gather | bytes 983040 | tf_op jit(solution)/shard_map/all_gather | solution.py:31
  215.3 1.0 fusion.11
  216.4 1.0 fusion.1
  217.4 0.8 copy-done.3
  218.2 1.7 convolution_convert_fusion
  220.0 84.7 %reduce-scatter.11.cloned.1.call-done = f32[256,704]{0,1:T(8,128)} async-done(((f32[2048,704]{0,1:T(8,128)}), f32[256,704]{0,1:T(8,128)}) %reduce-scatter.11.cloned.1.call-update) | async-done | bytes 720912 | tf_op jit(solution)/shard_map/reduce_scatter | solution.py:55
  304.7 2.1 bitcast_add_fusion
  306.8 194.0 %reduce-scatter.9.cloned.1.call-done = f32[256,1408]{0,1:T(8,128)} async-done(((f32[2048,1408]{0,1:T(8,128)}), f32[256,1408]{0,1:T(8,128)}) %reduce-scatter.9.cloned.1.call-update) | async-done | bytes 1441808 | tf_op jit(solution)/shard_map/reduce_scatter | solution.py:61
  500.8 2.6 fusion.2
  503.4 22.7 %reduce-scatter.7.cloned.1.call-done = bf16[48,2048]{1,0:T(8,128)(2,1)} async-done(((bf16[192,2048]{1,0:T(8,128)(2,1)}), bf16[48,2048]{1,0:T(8,128)(2,1)}) %reduce-scatter.7.cloned.1.call-update) | async-done | bytes 196624 | tf_op jit(solution)/shard_map/reduce_scatter | solution.py:69
  526.1 26.4 %reduce-scatter.5.cloned.1.call-done = bf16[48,2048]{1,0:T(8,128)(2,1)} async-done(((bf16[192,2048]{1,0:T(8,128)(2,1)}), bf16[48,2048]{1,0:T(8,128)(2,1)}) %reduce-scatter.5.cloned.1.call-update) | async-done | bytes 196624 | tf_op jit(solution)/shard_map/reduce_scatter | solution.py:35
  (22 shorter events, 0.2 us)
Async XLA Ops:
  7.2 65.2 %all-gather.4.cloned.1.call-start = ((), (), s32[]{:S(2)}) async-start(), calls=%async_computation.4 | async-start | bytes 3244032 | tf_op jit(solution)/shard_map/all_gather | solution.py:26
  7.9 124.2 %all-gather.6.cloned.1.call-start = ((), (), s32[]{:S(2)}) async-start(), calls=%async_computation.5 | async-start | bytes 3244032 | tf_op jit(solution)/shard_map/all_gather | solution.py:27
  8.6 183.3 %all-gather.8.cloned.1.call-start = ((), (), s32[]{:S(2)}) async-start(), calls=%async_computation.6 | async-start | bytes 3244032 | tf_op jit(solution)/shard_map/all_gather | solution.py:28
  9.4 295.3 %reduce-scatter.11.cloned.1.call-start = ((), (), s32[]{:S(2)}) async-start(), calls=%async_computation.10 | async-start | bytes 6488064 | tf_op jit(solution)/shard_map/reduce_scatter | solution.py:55
  138.4 362.3 %reduce-scatter.9.cloned.1.call-start = ((), (), s32[]{:S(2)}) async-start(), calls=%async_computation.9 | async-start | bytes 12976128 | tf_op jit(solution)/shard_map/reduce_scatter | solution.py:61
  201.0 1.8 copy-start
  201.1 325.0 %reduce-scatter.7.cloned.1.call-start = ((), (), s32[]{:S(2)}) async-start(), calls=%async_computation.8 | async-start | bytes 983040 | tf_op jit(solution)/shard_map/reduce_scatter | solution.py:69
  202.9 1.8 copy-start.1
  204.7 1.8 copy-start.8
  206.5 346.0 %reduce-scatter.5.cloned.1.call-start = ((), (), s32[]{:S(2)}) async-start(), calls=%async_computation.7 | async-start | bytes 983040 | tf_op jit(solution)/shard_map/reduce_scatter | solution.py:35
  206.5 9.8 %copy-start.2 = (bf16[2048,704]{0,1:T(8,128)(2,1)S(1)}, bf16[2048,704]{0,1:T(8,128)(2,1)}, u32[]{:S(2)}) copy-start(bf16[2048,704]{0,1:T(8,128)(2,1)} %all-gather.6.cloned.1.call-done) | copy-start | bytes 8650756
  216.4 1.9 copy-start.3
  218.2 88.5 %copy-start.7 = (bf16[192,704]{1,0:T(8,128)(2,1)}, bf16[192,704]{1,0:T(8,128)(2,1)S(1)}, u32[]{:S(2)}) copy-start(bf16[192,704]{1,0:T(8,128)(2,1)S(1)} %fusion.1) | copy-start | bytes 811012
  218.2 86.5 %copy-start.4 = (f32[704,256]{1,0:T(8,128)S(1)}, f32[704,256]{1,0:T(8,128)}, u32[]{:S(2)}) copy-start(f32[704,256]{1,0:T(8,128)} %param.17) | copy-start | bytes 2162692
  218.2 282.5 %copy-start.5 = (f32[256,704]{0,1:T(8,128)S(1)}, f32[256,704]{0,1:T(8,128)}, u32[]{:S(2)}) copy-start(f32[256,704]{0,1:T(8,128)} %param.16) | copy-start | bytes 2162692
  218.2 282.5 %copy-start.6 = (f32[256,704]{0,1:T(8,128)S(1)}, f32[256,704]{0,1:T(8,128)}, u32[]{:S(2)}) copy-start(f32[256,704]{0,1:T(8,128)} %param.15) | copy-start | bytes 2162692
Sparse Core Ops, SparseCore 0:
  10.0 62.2 all-gather.3
  74.4 57.7 all-gather.5
  134.2 57.7 all-gather.7
  195.5 109.1 reduce-scatter.10
  308.2 192.5 reduce-scatter.8
  503.7 22.2 reduce-scatter.6
  529.2 23.2 reduce-scatter.4
where the time goes:
time: 560 us; the launch traced here: 559 us
  waiting for transfers between devices  484 us (86%)
  blocking collectives  28 us (5%)
  matrix products  24.5 us (4%)
  between operations  14.2 us (3%)
    reduce_scatter x1, waiting for transfers between devices, local(): lax.psum_scatter(contract_rows(columns, stacked), 'fs', scatter_dimension...  194 us
    reduce_scatter x1, waiting for transfers between devices, local(): lax.psum_scatter(contract_rows(columns, hidden_prev), 'fs', scatter_dimen...  84.7 us
    all_gather x1, waiting for transfers between devices, local(): lax.all_gather(up_w, 'fs', axis=0, tiled=True)  57 us
    all_gather x1, waiting for transfers between devices, local(): lax.all_gather(down_w, 'fs', axis=1, tiled=True)  53.5 us
    all_gather x1, waiting for transfers between devices, local(): lax.all_gather(gate_w, 'fs', axis=0, tiled=True)  43.7 us
    reduce_scatter x1, waiting for transfers between devices, local(): lax.psum_scatter(jnp.dot(hidden, down_full, preferred_element_type=jnp.fl...  26.4 us
    reduce_scatter x1, waiting for transfers between devices, local(): lax.psum_scatter((first + second).astype(jnp.bfloat16), 'tp', scatter_dim...  22.7 us
  transfers between devices with their start and end apart: 7, of which 7 were waited for; matrix products, arithmetic and copies ran while one was open for 5% of the time, Pallas kernels for 0%

commit v1 on v0

v1 whole, which is shorter than its diff:
```python
import math

import jax
import jax.numpy as jnp
from jax import lax
from jax.experimental import pallas as pl
from jax.experimental.pallas import tpu as pltpu
from jax.sharding import PartitionSpec as P

MESH = pl.DeviceIdType.MESH
ANY = pl.BlockSpec(memory_space=pl.ANY)


def columns_of(size):
    side = 1
    while 8 * side * side <= size and size % (2 * side) == 0:
        side *= 2
    return side


def contract_rows(left, right):
    return lax.dot_general(
        left, right, (((0,), (0,)), ((), ())), preferred_element_type=jnp.float32
    )


def contract_cols(left, right):
    return lax.dot_general(
        left, right, (((1,), (1,)), ((), ())), preferred_element_type=jnp.float32
    )


def remote(source, target, send, recv, device):
    return pltpu.make_async_remote_copy(
        src_ref=source, dst_ref=target, send_sem=send, recv_sem=recv,
        device_id=device, device_id_type=MESH,
    )


class Spread:
    def __init__(self, fs, owns, fulls, send, recv):
        self.ny = columns_of(fs)
        self.nz = fs // self.ny
        self.fs, self.owns, self.fulls = fs, owns, fulls
        self.send, self.recv = send, recv
        self.f, self.t = lax.axis_index("fs"), lax.axis_index("tp")
        self.z, self.y = self.f // self.ny, lax.rem(self.f, self.ny)

    def flows(self, w, f, source, up, down, act):
        full = self.fulls[w].at[f]

        def go(kind, z, y):
            act(remote(source, full, self.send.at[w, kind, f], self.recv.at[w, f],
                       (z * self.ny + y, self.t)))

        if up:
            pl.when(self.z + 1 < self.nz)(lambda: go(0, self.z + 1, self.y))
        if down:
            pl.when(self.z > 0)(lambda: go(1, self.z - 1, self.y))
        for k in range(1, self.ny):
            go(1 + k, self.z, lax.rem(self.y + k, self.ny))

    def start(self):
        for w, own in enumerate(self.owns):
            self.flows(w, self.f, own, True, True, lambda c: c.start())

    def arrived(self, w, f):
        full = self.fulls[w].at[f]
        remote(full, full, self.send.at[w, 0, f], self.recv.at[w, f],
               (self.f, self.t)).wait_recv()

    def relay(self, act, wait):
        for d in range(1, self.nz):
            for w in range(len(self.owns)):
                def from_below(w=w, d=d):
                    f = (self.z - d) * self.ny + self.y
                    if wait:
                        self.arrived(w, f)
                    self.flows(w, f, self.fulls[w].at[f], True, False, act)

                def from_above(w=w, d=d):
                    f = (self.z + d) * self.ny + self.y
                    if wait:
                        self.arrived(w, f)
                    self.flows(w, f, self.fulls[w].at[f], False, True, act)

                pl.when(self.z >= d)(from_below)
                pl.when(self.z + d < self.nz)(from_above)

    def finish(self):
        for w in range(len(self.owns)):
            for z in range(self.nz):
                for k in range(1, self.ny):
                    self.arrived(w, z * self.ny + lax.rem(self.y + k, self.ny))
        for w, own in enumerate(self.owns):
            self.flows(w, self.f, own, True, True, lambda c: c.wait_send())
        self.relay(lambda c: c.wait_send(), False)


def stage_in(pairs, sem):
    copies = [pltpu.make_async_copy(a, b, sem.at[i]) for i, (a, b) in enumerate(pairs)]
    for copy in copies:
        copy.start()
    return copies


def gather_inputs(fs, tp, *refs):
    (gate, up, down, xn, xp, go, cols,
     gate_o, up_o, down_o, xn_o, xp_o, go_o, cols_o,
     *rest) = refs
    held, (wsend, wrecv, tsend, trecv, csend, crecv, dsend, drecv, lin, lout) = rest[:7], rest[7:]
    f, t = lax.axis_index("fs"), lax.axis_index("tp")
    sources = (gate, up, down, xn, xp, go, cols)
    into = stage_in(list(zip(sources, held)), lin)
    spread = Spread(fs, held[:3], (gate_o, up_o, down_o), wsend, wrecv)
    for copy in into[:3]:
        copy.wait()
    spread.start()
    for copy in into[3:]:
        copy.wait()
    tokens = ((held[3], xn_o), (held[4], xp_o), (held[5], go_o))
    token_copies = [
        remote(a, b.at[t], tsend.at[i, k], trecv.at[i, t], (f, lax.rem(t + k, tp)))
        for i, (a, b) in enumerate(tokens) for k in range(1, tp)
    ]
    slices = held[6]
    slice_copies = []
    for k in range(1, fs):
        other = lax.rem(f + k, fs)
        slice_copies.append(
            remote(slices.at[other], cols_o.at[f, t], csend.at[k], crecv.at[f], (other, t)))
    for copy in token_copies + slice_copies:
        copy.start()
    out = stage_in(
        [(held[0], gate_o.at[f]), (held[1], up_o.at[f]), (held[2], down_o.at[f]),
         (held[3], xn_o.at[t]), (held[4], xp_o.at[t]), (held[5], go_o.at[t]),
         (slices.at[f], cols_o.at[f, t])], lout)
    spread.relay(lambda c: c.start(), True)
    out[6].wait()
    for k in range(1, fs):
        other = lax.rem(f + k, fs)
        mine = cols_o.at[other, t]
        remote(mine, mine, csend.at[k], crecv.at[other], (f, t)).wait_recv()
    mine = cols_o.at[:, t]
    share = [remote(mine, mine, dsend.at[k], drecv.at[t], (f, lax.rem(t + k, tp)))
             for k in range(1, tp)]
    for copy in share:
        copy.start()
    for k in range(1, tp):
        other = lax.rem(t + k, tp)
        for i, (_, b) in enumerate(tokens):
            remote(b.at[other], b.at[other], tsend.at[i, k], trecv.at[i, other], (f, t)).wait_recv()
        theirs = cols_o.at[:, other]
        remote(theirs, theirs, dsend.at[k], drecv.at[other], (f, t)).wait_recv()
    spread.finish()
    for copy in token_copies + slice_copies + share:
        copy.wait_send()
    for copy in out[:6]:
        copy.wait()


def gather_terms(fs, tp, *refs):
    (gg, gu, hp, pn, pp, gg_o, gu_o, hp_o, pn_o, pp_o, *rest) = refs
    held, (wsend, wrecv, tsend, trecv, lin, lout) = rest[:5], rest[5:]
    f, t = lax.axis_index("fs"), lax.axis_index("tp")
    into = stage_in(list(zip((gg, gu, hp, pn, pp), held)), lin)
    spread = Spread(fs, held[:3], (gg_o, gu_o, hp_o), wsend, wrecv)
    for copy in into[:3]:
        copy.wait()
    spread.start()
    for copy in into[3:]:
        copy.wait()
    parts = ((held[3], pn_o), (held[4], pp_o))
    part_copies = []
    for i, (a, b) in enumerate(parts):
        for k in range(1, tp):
            other = lax.rem(t + k, tp)
            part_copies.append(
                remote(a.at[other], b.at[t], tsend.at[i, k], trecv.at[i, t], (f, other)))
    for copy in part_copies:
        copy.start()
    out = stage_in(
        [(held[0], gg_o.at[f]), (held[1], gu_o.at[f]), (held[2], hp_o.at[f]),
         (held[3].at[t], pn_o.at[t]), (held[4].at[t], pp_o.at[t])], lout)
    spread.relay(lambda c: c.start(), True)
    for i, (_, b) in enumerate(parts):
        for k in range(1, tp):
            other = lax.rem(t + k, tp)
            remote(b.at[other], b.at[other], tsend.at[i, k], trecv.at[i, other], (f, t)).wait_recv()
    spread.finish()
    for copy in part_copies:
        copy.wait_send()
    for copy in out:
        copy.wait()


def communicate(body, fs, tp, args, shapes, extra, name):
    n = len(args)
    return pl.pallas_call(
        lambda *refs: body(fs, tp, *refs),
        out_shape=[jax.ShapeDtypeStruct(s, jnp.bfloat16) for s in shapes],
        in_specs=[ANY] * n,
        out_specs=[ANY] * len(shapes),
        scratch_shapes=[pltpu.VMEM(a.shape, a.dtype) for a in args]
        + [pltpu.SemaphoreType.DMA((3, columns_of(fs) + 1, fs)), pltpu.SemaphoreType.DMA((3, fs)),
           pltpu.SemaphoreType.DMA((3, tp)), pltpu.SemaphoreType.DMA((3, tp))]
        + extra
        + [pltpu.SemaphoreType.DMA((n,)), pltpu.SemaphoreType.DMA((n,))],
        compiler_params=pltpu.CompilerParams(has_side_effects=True),
        name=name,
    )(*args)


def local(x_next, x_prev, grad_out, gate_w, up_w, down_w, acc_gate, acc_up, acc_down):
    fs, tp = lax.axis_size("fs"), lax.axis_size("tp")
    rows, model = x_prev.shape
    depth, width = gate_w.shape
    factor = 1.0 / math.sqrt(rows * tp * fs)
    cols = jnp.concatenate(
        (x_prev.reshape(rows, fs, depth), grad_out.reshape(rows, fs, depth)), axis=2
    ).transpose(1, 0, 2)
    sems = pltpu.SemaphoreType.DMA
    gate_full, up_full, down_full, piece, rows_prev, cotangent, all_cols = communicate(
        gather_inputs, fs, tp, (gate_w, up_w, down_w, x_next, x_prev, grad_out, cols),
        [(fs, depth, width), (fs, depth, width), (fs, width, depth)]
        + [(tp, rows, model)] * 3 + [(fs, tp, rows, 2 * depth)],
        [sems((fs,)), sems((fs,)), sems((tp,)), sems((tp,))], "gather_inputs",
    )
    gate_full, up_full = gate_full.reshape(model, width), up_full.reshape(model, width)
    down_full = down_full.transpose(1, 0, 2).reshape(width, model)
    piece, rows_prev, cotangent = (a.reshape(tp * rows, model) for a in (piece, rows_prev, cotangent))
    x_cols = all_cols[..., :depth].reshape(fs * tp * rows, depth)
    g_cols = all_cols[..., depth:].reshape(fs * tp * rows, depth)

    gate = jnp.dot(piece, gate_full, preferred_element_type=jnp.float32)
    upper = jnp.dot(piece, up_full, preferred_element_type=jnp.float32)
    hidden = (jax.nn.silu(gate) * upper).astype(jnp.bfloat16)
    part_next = jnp.dot(hidden, down_full, preferred_element_type=jnp.float32).astype(jnp.bfloat16)
    gate_prev = jnp.dot(rows_prev, gate_full, preferred_element_type=jnp.float32)
    up_prev = jnp.dot(rows_prev, up_full, preferred_element_type=jnp.float32)
    grad_hidden = contract_cols(cotangent, down_full)
    sigmoid_gate = jax.nn.sigmoid(gate_prev)
    silu_gate = gate_prev * sigmoid_gate
    grad_gate = (
        grad_hidden * up_prev * sigmoid_gate * (1.0 + gate_prev * (1.0 - sigmoid_gate))
    ).astype(jnp.bfloat16)
    grad_up = (grad_hidden * silu_gate).astype(jnp.bfloat16)
    hidden_prev = (silu_gate * up_prev).astype(jnp.bfloat16)
    part_prev = (contract_cols(grad_gate, gate_full) + contract_cols(grad_up, up_full)).astype(jnp.bfloat16)

    all_gate, all_up, all_hidden, parts_next, parts_prev = communicate(
        gather_terms, fs, tp,
        (grad_gate, grad_up, hidden_prev,
         part_next.reshape(tp, rows, model), part_prev.reshape(tp, rows, model)),
        [(fs, tp * rows, width)] * 3 + [(tp, rows, model)] * 2, [], "gather_terms",
    )
    all_gate, all_up, all_hidden = (a.reshape(fs * tp * rows, width) for a in (all_gate, all_up, all_hidden))
    new_gate = acc_gate + factor * contract_rows(x_cols, all_gate)
    new_up = acc_up + factor * contract_rows(x_cols, all_up)
    new_down = acc_down + factor * contract_rows(all_hidden, g_cols)
    summed = parts_next.astype(jnp.float32).sum(0).astype(jnp.bfloat16)
    grad_input = parts_prev.astype(jnp.float32).sum(0).astype(jnp.bfloat16)
    return (summed, hidden, grad_input, new_gate, new_up, new_down)


def solution(mesh):
    in_specs = (
        P(("fs", "tp"), None),
        P(("fs", "tp"), None),
        P(("fs", "tp"), None),
        P("fs", "tp"),
        P("fs", "tp"),
        P("tp", "fs"),
        P("fs", "tp"),
        P("fs", "tp"),
        P("tp", "fs"),
    )
    out_specs = (
        P(("fs", "tp"), None),
        P("fs", "tp"),
        P(("fs", "tp"), None),
        P("fs", "tp"),
        P("fs", "tp"),
        P("tp", "fs"),
    )
    return jax.shard_map(local, mesh=mesh, in_specs=in_specs, out_specs=out_specs, check_vma=False)
```

time: 560 us -> 234 us (0.42)
  waiting for transfers between devices: 484 us -> 0 us
  Pallas kernels: 0 us -> 201 us
  blocking collectives: 28 us -> 0 us
  between operations: 14.2 us -> 0.78 us
  local copies, waits for them, and re-layouts: 3.63 us -> 9.44 us
    reduce_scatter x4 -> x0, waiting for transfers between devices: 328 us -> none  [the longest x1 194 us: local(): lax.psum_scatter(contract_rows(columns, stacked), 'fs', scatter_dimension...]
    pallas_call x0 -> x2, Pallas kernels: none -> 201 us  [communicate(): pl.pallas_call(lambda *refs: body(fs, tp, *refs), out_shape=[jax.ShapeDty...]
    all_gather x3 -> x0, waiting for transfers between devices: 154 us -> none  [the longest x1 57 us: local(): lax.all_gather(up_w, 'fs', axis=0, tiled=True)]
    all_gather x3 -> x0, blocking collectives: 28 us -> none  [the longest x1 10.3 us: local(): rows_prev = lax.all_gather(x_prev, 'tp', axis=0, tiled=True)]
  transfers between devices with their start and end apart: 7 -> 0, of which waited for: 7 -> 0; matrix products, arithmetic and copies ran while one was open for 5% -> 0% of each run, Pallas kernels for 0% -> 0%
where the time goes in v1:
time: 234 us
  Pallas kernels  201 us (86%)
  matrix products  19.2 us (8%)
  local copies, waits for them, and re-layouts  9.44 us (4%)
  other arithmetic  3.74 us (2%)
    pallas_call x2, Pallas kernels, communicate(): pl.pallas_call(lambda *refs: body(fs, tp, *refs), out_shape=[jax.ShapeDty...  201 us
    dot_general x3, matrix products, contract_rows(): lax.dot_general(left, right, (((0,), (0,)), ((), ())), preferred_element_...  9.04 us
    unnamed x28, local copies, waits for them, and re-layouts  5.97 us

profile of v1, /device:TPU:0, one launch (start us, length us, event | category | flops | bytes accessed | tf_op | source)
XLA Modules:
  0.0 234.0 jit_solution(2353610793996042800)
XLA Ops:
  0.6 1.9 copy.19.refs_0_
  2.5 1.9 copy.20.refs_1_
  4.4 1.0 copy_bitcast_fusion
  5.5 0.8 maximum_bitcast_fusion.refs_6_
  6.3 115.3 %gather_inputs.1 = (bf16[8,256,704]{2,1,0:T(8,128)(2,1)}, bf16[8,256,704]{2,1,0:T(8,128)(2,1)}, bf16[8,704,256]{2,1,0:T(8,128)(2,1)}, bf16[4,48,2048]{2,1,0:T(8,...) custom-call(bf16[256,704]{1,0:T(8,128)(2,1)} %copy.19.refs_0_, ...), custom_call_target="tpu_custom_call" | custom-call | tf_op jit(solution)/shard_map/gather_inputs/pallas_call | solution.py:199
  121.6 0.0 copy-start.6
  121.6 2.3 copy.24
  123.8 0.0 copy-start
  123.9 0.0 copy-start.9
  123.9 0.0 copy-done.6
  123.9 1.0 fusion.7
  124.9 0.8 copy-done
  125.7 0.2 copy-done.9
  125.9 0.8 fusion.8
  126.7 1.1 copy-done.1
  127.8 1.7 multiply_convert_fusion
  129.5 0.0 copy-done.8
  129.5 0.8 fusion.9
  130.3 1.2 fusion.10
  131.5 0.0 copy-done.4
  131.5 0.8 fusion.4
  132.3 0.0 copy-start.11
  132.3 2.2 fusion
  134.5 0.0 copy-done.11
  134.5 1.7 convolution_convert_fusion
  136.2 0.2 fusion.6
  136.4 85.6 %gather_terms.1 = (bf16[8,192,704]{2,1,0:T(8,128)(2,1)}, bf16[8,192,704]{2,1,0:T(8,128)(2,1)}, bf16[8,192,704]{2,1,0:T(8,128)(2,1)}, bf16[4,48,2048]{2,1,0:T(8,128)(2,1)}, bf16[4,48,2048]{2,1,0:T(8,128)(2,1)}) custom-call(bf16[192,704]{1,0:T(8,128)(2,1)} %copy-done.4, bf16[192,704]{1,0:T(8,128)(2,1)} %copy-done.5, ...), custom_call_target="tpu_custom_call" | custom-call | tf_op jit(solution)/shard_map/gather_terms/pallas_call | solution.py:199
  222.0 3.4 %fusion.1 = f32[704,256]{1,0:T(8,128)} fusion(f32[704,256]{1,0:T(8,128)S(1)} %copy-done.12, bf16[1536,704]{1,0:T(8,128)(2,1)} %bitcast.68, bf16[1536,256]{1,0:T(8,128)(2,1)S(1)} %bitcast.63), kind=kOutput, calls=%fused_computation.4 | convolution fusion | flops 554008576 | bytes 4390912 | tf_op jit(solution)/shard_map/dot_general | solution.py:22
  225.4 0.8 reduce_sum.24
  226.2 2.1 reduce_sum.25
  228.4 3.8 %fusion.3 = f32[256,704]{0,1:T(8,128)} fusion(f32[256,704]{0,1:T(8,128)} %param.15, bf16[1536,256]{1,0:T(8,128)(2,1)S(1)} %bitcast.50, bf16[1536,704]{1,0:T(8,128)(2,1)} %bitcast.59), kind=kOutput, calls=%fused_computation.8 | convolution fusion | flops 554008576 | bytes 4390912 | tf_op jit(solution)/shard_map/dot_general | solution.py:22
  232.1 1.9 fusion.2
  (15 shorter events, 0.0 us)
Async XLA Ops:
  121.6 2.3 copy-start.6
  123.8 1.9 copy-start
  123.9 2.1 copy-start.9
  125.9 1.9 copy-start.1
  127.8 1.7 copy-start.8
  129.5 2.0 copy-start.4
  129.5 2.8 %copy-start.5 = (bf16[192,704]{1,0:T(8,128)(2,1)}, bf16[192,704]{1,0:T(8,128)(2,1)S(1)}, u32[]{:S(2)}) copy-start(bf16[192,704]{1,0:T(8,128)(2,1)S(1)} %get-tuple-element.34.refs_1_) | copy-start | bytes 811012
  132.3 2.2 copy-start.11
  134.5 1.7 copy-start.3
  136.2 85.8 %copy-start.12 = (f32[704,256]{1,0:T(8,128)S(1)}, f32[704,256]{1,0:T(8,128)}, u32[]{:S(2)}) copy-start(f32[704,256]{1,0:T(8,128)} %param.17) | copy-start | bytes 2162692
  222.0 3.4 %copy-start.7 = (bf16[4,48,2048]{2,1,0:T(8,128)(2,1)S(1)}, bf16[4,48,2048]{2,1,0:T(8,128)(2,1)}, u32[]{:S(2)}) copy-start(bf16[4,48,2048]{2,1,0:T(8,128)(2,1)} %get-tuple-element.24) | copy-start | bytes 2359300
  226.2 5.9 %copy-start.2 = (bf16[8,192,704]{2,1,0:T(8,128)(2,1)S(1)}, bf16[8,192,704]{2,1,0:T(8,128)(2,1)}, u32[]{:S(2)}) copy-start(bf16[8,192,704]{2,1,0:T(8,128)(2,1)} %get-tuple-element.28) | copy-start | bytes 6488068
  228.4 3.8 %copy-start.10 = (f32[256,704]{0,1:T(8,128)S(1)}, f32[256,704]{0,1:T(8,128)}, u32[]{:S(2)}) copy-start(f32[256,704]{0,1:T(8,128)} %param.16) | copy-start | bytes 2162692

commit v2 on v1

--- a/solution.py
+++ b/solution.py
@@ -221,23 +221,22 @@
     ).transpose(1, 0, 2)
     sems = pltpu.SemaphoreType.DMA
     gate_full, up_full, down_full, piece, rows_prev, cotangent, all_cols = communicate(
-        gather_inputs, fs, tp, (gate_w, up_w, down_w, x_next, x_prev, grad_out, cols),
-        [(fs, depth, width), (fs, depth, width), (fs, width, depth)]
+        gather_inputs, fs, tp, (gate_w.T, up_w.T, down_w, x_next, x_prev, grad_out, cols),
+        [(fs, width, depth)] * 3
         + [(tp, rows, model)] * 3 + [(fs, tp, rows, 2 * depth)],
         [sems((fs,)), sems((fs,)), sems((tp,)), sems((tp,))], "gather_inputs",
     )
-    gate_full, up_full = gate_full.reshape(model, width), up_full.reshape(model, width)
-    down_full = down_full.transpose(1, 0, 2).reshape(width, model)
+    gate_full, up_full, down_full = (
+        a.transpose(1, 0, 2).reshape(width, model) for a in (gate_full, up_full, down_full)
+    )
     piece, rows_prev, cotangent = (a.reshape(tp * rows, model) for a in (piece, rows_prev, cotangent))
     x_cols = all_cols[..., :depth].reshape(fs * tp * rows, depth)
     g_cols = all_cols[..., depth:].reshape(fs * tp * rows, depth)
 
-    gate = jnp.dot(piece, gate_full, preferred_element_type=jnp.float32)
-    upper = jnp.dot(piece, up_full, preferred_element_type=jnp.float32)
+    gate, upper = contract_cols(piece, gate_full), contract_cols(piece, up_full)
     hidden = (jax.nn.silu(gate) * upper).astype(jnp.bfloat16)
     part_next = jnp.dot(hidden, down_full, preferred_element_type=jnp.float32).astype(jnp.bfloat16)
-    gate_prev = jnp.dot(rows_prev, gate_full, preferred_element_type=jnp.float32)
-    up_prev = jnp.dot(rows_prev, up_full, preferred_element_type=jnp.float32)
+    gate_prev, up_prev = contract_cols(rows_prev, gate_full), contract_cols(rows_prev, up_full)
     grad_hidden = contract_cols(cotangent, down_full)
     sigmoid_gate = jax.nn.sigmoid(gate_prev)
     silu_gate = gate_prev * sigmoid_gate
@@ -246,7 +245,10 @@
     ).astype(jnp.bfloat16)
     grad_up = (grad_hidden * silu_gate).astype(jnp.bfloat16)
     hidden_prev = (silu_gate * up_prev).astype(jnp.bfloat16)
-    part_prev = (contract_cols(grad_gate, gate_full) + contract_cols(grad_up, up_full)).astype(jnp.bfloat16)
+    part_prev = (
+        jnp.dot(grad_gate, gate_full, preferred_element_type=jnp.float32)
+        + jnp.dot(grad_up, up_full, preferred_element_type=jnp.float32)
+    ).astype(jnp.bfloat16)
 
     all_gate, all_up, all_hidden, parts_next, parts_prev = communicate(
         gather_terms, fs, tp,

time: 234 us -> 227 us (0.970)
  Pallas kernels: 201 us -> 195 us
    pallas_call x2, Pallas kernels: 201 us -> 195 us  [communicate(): pl.pallas_call(lambda *refs: body(fs, tp, *refs), out_shape=[jax.ShapeDty...]
    unnamed x28 -> x26, local copies, waits for them, and re-layouts: 5.97 us -> 3.32 us
    dot_general x3 -> x5, matrix products: 4.36 us -> 5.95 us  [contract_cols(): lax.dot_general(left, right, (((1,), (1,)), ((), ())), preferred_element_...]
where the time goes in v2:
time: 227 us
  Pallas kernels  195 us (86%)
  matrix products  19.3 us (9%)
  local copies, waits for them, and re-layouts  7.55 us (3%)
  other arithmetic  3.74 us (2%)
    pallas_call x2, Pallas kernels, communicate(): pl.pallas_call(lambda *refs: body(fs, tp, *refs), out_shape=[jax.ShapeDty...  195 us
    dot_general x3, matrix products, contract_rows(): lax.dot_general(left, right, (((0,), (0,)), ((), ())), preferred_element_...  9.04 us
    dot_general x5, matrix products, contract_cols(): lax.dot_general(left, right, (((1,), (1,)), ((), ())), preferred_element_...  5.95 us

profile of v2, /device:TPU:0, one launch (start us, length us, event | category | flops | bytes accessed | tf_op | source)
XLA Modules:
  0.0 226.6 jit_solution(10953483635780078426)
XLA Ops:
  0.6 1.1 copy_bitcast_fusion
  1.7 0.8 maximum_bitcast_fusion.refs_6_
  2.5 109.6 %gather_inputs.1 = (bf16[8,704,256]{2,1,0:T(8,128)(2,1)}, bf16[8,704,256]{2,1,0:T(8,128)(2,1)}, bf16[8,704,256]{2,1,0:T(8,128)(2,1)}, bf16[4,48,2048]{2,1,0:T(8,...) custom-call(bf16[704,256]{1,0:T(8,128)(2,1)} %bitcast.76, ...), custom_call_target="tpu_custom_call" | custom-call | tf_op jit(solution)/shard_map/gather_inputs/pallas_call | solution.py:199
  112.1 0.0 copy-start.8
  112.1 2.3 %copy.22 = bf16[8,88,8,256]{3,2,0,1:T(8,128)(2,1)S(1)} copy(bf16[8,88,8,256]{3,2,1,0:T(8,128)(2,1)} %bitcast.65) | data formatting | bytes 5767168 | tf_op jit(solution)/shard_map/reshape | solution.py:230
  114.4 0.0 copy-start.4
  114.4 0.0 copy-done.8
  114.4 1.0 fusion.7
  115.5 0.4 copy-done.4
  115.8 0.2 fusion.6
  116.0 0.7 copy-done.1
  116.7 0.4 copy.23
  117.1 1.4 copy-done
  118.5 0.4 copy.24
  118.9 0.7 copy-done.7
  119.7 1.0 fusion.9
  120.7 1.0 fusion.4
  121.7 0.0 copy-start.11
  121.8 1.7 convolution_convert_fusion
  123.5 1.0 fusion.8
  124.5 1.9 multiply_convert_fusion
  126.4 0.8 fusion.10
  127.2 0.0 copy-start.12
  127.2 1.8 fusion
  129.0 85.6 %gather_terms.1 = (bf16[8,192,704]{2,1,0:T(8,128)(2,1)}, bf16[8,192,704]{2,1,0:T(8,128)(2,1)}, bf16[8,192,704]{2,1,0:T(8,128)(2,1)}, bf16[4,48,2048]{2,1,0:T(8,128)(2,1)}, bf16[4,48,2048]{2,1,0:T(8,128)(2,1)}) custom-call(bf16[192,704]{1,0:T(8,128)(2,1)} %copy-done.5, bf16[192,704]{1,0:T(8,128)(2,1)} %copy-done.3, ...), custom_call_target="tpu_custom_call" | custom-call | tf_op jit(solution)/shard_map/gather_terms/pallas_call | solution.py:199
  214.6 3.4 %fusion.1 = f32[704,256]{1,0:T(8,128)} fusion(f32[704,256]{1,0:T(8,128)S(1)} %copy-done.12, bf16[1536,704]{1,0:T(8,128)(2,1)} %bitcast.78, bf16[1536,256]{1,0:T(8,128)(2,1)S(1)} %bitcast.73), kind=kOutput, calls=%fused_computation.4 | convolution fusion | flops 554008576 | bytes 4390912 | tf_op jit(solution)/shard_map/dot_general | solution.py:22
  218.0 0.0 copy-done.9
  218.0 0.8 reduce_sum.24
  218.8 2.1 reduce_sum.25
  220.9 3.8 %fusion.3 = f32[256,704]{0,1:T(8,128)} fusion(f32[256,704]{0,1:T(8,128)} %param.15, bf16[1536,256]{1,0:T(8,128)(2,1)S(1)} %bitcast.59, bf16[1536,704]{1,0:T(8,128)(2,1)} %bitcast.67), kind=kOutput, calls=%fused_computation.8 | convolution fusion | flops 554008576 | bytes 4390912 | tf_op jit(solution)/shard_map/dot_general | solution.py:22
  224.7 0.0 copy-done.10
  224.7 1.9 fusion.2
  (15 shorter events, 0.0 us)
Async XLA Ops:
  112.1 2.3 %copy-start.8 = (bf16[4,48,2048]{2,1,0:T(8,128)(2,1)S(1)}, bf16[4,48,2048]{2,1,0:T(8,128)(2,1)}, u32[]{:S(2)}) copy-start(bf16[4,48,2048]{2,1,0:T(8,128)(2,1)} %get-tuple-element.18) | copy-start | bytes 2359300
  114.4 1.4 copy-start.4
  114.4 2.3 %copy-start.1 = (bf16[8,704,256]{2,1,0:T(8,128)(2,1)S(1)}, bf16[8,704,256]{2,1,0:T(8,128)(2,1)}, u32[]{:S(2)}) copy-start(bf16[8,704,256]{2,1,0:T(8,128)(2,1)} %get-tuple-element.21) | copy-start | bytes 8650756
  116.7 1.8 copy-start
  118.5 1.1 copy-start.7
  121.7 2.8 %copy-start.11 = (bf16[192,704]{1,0:T(8,128)(2,1)}, bf16[192,704]{1,0:T(8,128)(2,1)S(1)}, u32[]{:S(2)}) copy-start(bf16[192,704]{1,0:T(8,128)(2,1)S(1)} %fusion.4) | copy-start | bytes 811012
  121.8 1.7 copy-start.6
  126.4 2.6 %copy-start.3 = (bf16[192,704]{1,0:T(8,128)(2,1)}, bf16[192,704]{1,0:T(8,128)(2,1)S(1)}, u32[]{:S(2)}) copy-start(bf16[192,704]{1,0:T(8,128)(2,1)S(1)} %get-tuple-element.34.refs_1_) | copy-start | bytes 811012
  126.4 2.6 %copy-start.5 = (bf16[192,704]{1,0:T(8,128)(2,1)}, bf16[192,704]{1,0:T(8,128)(2,1)S(1)}, u32[]{:S(2)}) copy-start(bf16[192,704]{1,0:T(8,128)(2,1)S(1)} %get-tuple-element.33.refs_0_) | copy-start | bytes 811012
  127.2 87.4 %copy-start.12 = (f32[704,256]{1,0:T(8,128)S(1)}, f32[704,256]{1,0:T(8,128)}, u32[]{:S(2)}) copy-start(f32[704,256]{1,0:T(8,128)} %param.17) | copy-start | bytes 2162692
  214.6 3.4 %copy-start.9 = (bf16[4,48,2048]{2,1,0:T(8,128)(2,1)S(1)}, bf16[4,48,2048]{2,1,0:T(8,128)(2,1)}, u32[]{:S(2)}) copy-start(bf16[4,48,2048]{2,1,0:T(8,128)(2,1)} %get-tuple-element.24) | copy-start | bytes 2359300
  218.8 5.9 %copy-start.2 = (bf16[8,192,704]{2,1,0:T(8,128)(2,1)S(1)}, bf16[8,192,704]{2,1,0:T(8,128)(2,1)}, u32[]{:S(2)}) copy-start(bf16[8,192,704]{2,1,0:T(8,128)(2,1)} %get-tuple-element.28) | copy-start | bytes 6488068
  220.9 3.8 %copy-start.10 = (f32[256,704]{0,1:T(8,128)S(1)}, f32[256,704]{0,1:T(8,128)}, u32[]{:S(2)}) copy-start(f32[256,704]{0,1:T(8,128)} %param.16) | copy-start | bytes 2162692
